TPU v7x, 256 devices: a whole 4x4x8 slice. The times are simulated.
256 devices in a mesh: ep: 64 (over z, y, core), tp: 4 (over x).
Axes of the slice: x: 4, y: 4, z: 8, core: 2. Of those that a mesh axis runs over, the one named last changes fastest.
Arguments:
- first_input: bfloat16 [32768, 2048], P('ep'), may hold values from -120 to 120
- first_gain: bfloat16 [2048], replicated, may hold values from 0.099609375 to 1.8984375
- pool_inward: bfloat16 [2048, 1024], P(None, 'tp'), may hold values from -0.125 to 0.125
- pool_mixing: bfloat16 [4, 256, 256], P('tp'), may hold values from -0.375 to 0.375
- pool_scale: bfloat16 [1024], P('tp'), may hold values from 0.099609375 to 1.8984375
- pool_outward: bfloat16 [1024, 2048], P('tp'), may hold values from -0.1875 to 0.1875
- second_input: bfloat16 [16384, 2048], P('ep'), may hold values from -120 to 120
- second_gain: bfloat16 [2048], replicated, may hold values from 0.099609375 to 1.8984375
- route_ids: int32 [16384, 2], P('ep'), may hold values from 0 to 31, all different within a row; in each aligned block of 256 rows (0 to 255, 256 to 511, ...) at most 18 rows name the same one
- route_logits: float32 [16384, 2], P('ep'), may hold values from -6 to 6
- expert_gate: bfloat16 [64, 2048, 2048], P('ep', None, 'tp'), may hold values from -0.125 to 0.125
- expert_up: bfloat16 [64, 2048, 2048], P('ep', None, 'tp'), may hold values from -0.125 to 0.125
- expert_down: bfloat16 [64, 2048, 2048], P('ep', 'tp'), may hold values from -0.09375 to 0.09375
Outputs:
- first_out: bfloat16 [32768, 2048], P('ep', 'tp')
- second_out: bfloat16 [16384, 2048], P('ep', 'tp')
Inputs may be any that keep to these rules, and one draw needn't show every extreme that they name: `route_ids`: each row names two different experts. In each aligned block of 256 rows (the rows of one index of ep) no expert is named by more than 18 rows, and in some blocks one expert is named by exactly 18 rows.
All inputs are finite; a program needn't handle non-finite values.
Results may differ from a plain program's by a relative error of at most 0.012.
Values may be sent and summed in bfloat16 or wider, within the bound.
No kernel may reach another device: no remote copies, remote signals or barrier semaphores. Data moves between devices by JAX's collectives and lax.ppermute only.
A program may use at most 64 MiB of HBM per device.

v0:
```python
import jax
import jax.numpy as jnp
from jax import lax
from jax.sharding import Mesh, PartitionSpec as P

epsilon = 1e-06


def from_behind(value, axis, steps):
    count = lax.axis_size(axis)
    leading, last = (max(0, -steps), min(count, count - steps))
    return lax.ppermute(value, axis, [(source, source + steps) for source in range(leading, last)])


def rms_scaled(values, weights):
    widened = values.astype(jnp.float32)
    inverse = lax.rsqrt(jnp.mean(widened * widened, axis=-1, keepdims=True) + epsilon)
    return (widened * inverse * weights.astype(jnp.float32)).astype(jnp.bfloat16)


def window_means(channels, length, offset):
    row_count = channels.shape[0] - 15
    summed = jnp.zeros((row_count, channels.shape[1]), jnp.float32)
    for lookback in range(16):
        summed = summed + jnp.where(
            lookback < length, channels[15 - lookback : 15 - lookback + row_count], 0.0
        )
    positions = offset + jnp.arange(row_count, dtype=jnp.int32)
    counts = jnp.minimum(positions + 1, length).astype(jnp.float32)
    return summed / counts[:, None]


def slot_positions(block_ids, expert_count, capacity):
    flattened = block_ids.reshape(-1)
    onehot = (flattened[:, None] == jnp.arange(expert_count, dtype=jnp.int32)[None, :]).astype(
        jnp.int32
    )
    running = jnp.cumsum(onehot, axis=0, dtype=jnp.int32) - 1
    slot_numbers = jnp.sum(onehot * running, axis=1)
    return flattened * capacity + slot_numbers


def expert_output(gate_sum, up_sum, down_rows):
    hidden = (jax.nn.silu(gate_sum) * up_sum).astype(jnp.bfloat16)
    return jnp.dot(hidden, down_rows, preferred_element_type=jnp.float32)


def local(
    first_input,
    first_gain,
    pool_inward,
    pool_mixing,
    pool_scale,
    pool_outward,
    second_input,
    second_gain,
    route_ids,
    route_logits,
    expert_gate,
    expert_up,
    expert_down,
):
    tensor_parts = lax.axis_size("tp")
    expert_count = lax.axis_size("z") * lax.axis_size("y")
    model_width = first_input.shape[1]
    quarter_width = model_width // tensor_parts
    swap = [(0, 1), (1, 0)]
    gate_other = lax.ppermute(expert_gate[0], "core", swap)
    up_other = lax.ppermute(expert_up[0], "core", swap)
    down_other = lax.ppermute(expert_down[0], "core", swap)
    normed_first = rms_scaled(first_input, first_gain)
    pooled_in = jnp.dot(normed_first, pool_inward, preferred_element_type=jnp.float32).astype(
        jnp.bfloat16
    )
    halo_rows = from_behind(pooled_in[-15:], ("z", "y", "core"), 1)
    extended = jnp.concatenate([halo_rows, pooled_in], axis=0).astype(jnp.float32)
    window = jnp.left_shift(jnp.int32(2), lax.axis_index("tp"))
    sequence_start = lax.axis_index(("z", "y", "core")) * first_input.shape[0]
    means = window_means(extended, window, sequence_start)
    mixed = (means - pooled_in.astype(jnp.float32)).astype(jnp.bfloat16)
    pooled = (
        jnp.dot(mixed, pool_mixing[0], preferred_element_type=jnp.float32)
        * pool_scale.astype(jnp.float32)
    ).astype(jnp.bfloat16)
    mixer_term = jnp.dot(pooled, pool_outward, preferred_element_type=jnp.float32)
    normed_second = rms_scaled(second_input, second_gain)
    row_count = second_input.shape[0]
    capacity = 2 * row_count * 9 // (8 * expert_count)
    positions = slot_positions(route_ids, expert_count, capacity)
    quarter = lax.dynamic_slice_in_dim(
        normed_second, lax.axis_index("tp") * quarter_width, quarter_width, 1
    )
    repeated = jnp.repeat(quarter, 2, axis=0)
    buffer = (
        jnp.zeros((expert_count * capacity, quarter_width), jnp.bfloat16)
        .at[positions]
        .set(repeated)
        .reshape(expert_count, capacity, quarter_width)
    )
    arrived = lax.all_to_all(buffer, ("z", "y"), split_axis=0, concat_axis=0, tiled=True)
    flattened = arrived.reshape(-1, quarter_width)
    portion = lax.all_gather(flattened, "tp", axis=1, tiled=True)
    flat_term = expert_output(
        jnp.dot(portion, expert_gate[0], preferred_element_type=jnp.float32),
        jnp.dot(portion, expert_up[0], preferred_element_type=jnp.float32),
        expert_down[0],
    ) + expert_output(
        jnp.dot(portion, gate_other, preferred_element_type=jnp.float32),
        jnp.dot(portion, up_other, preferred_element_type=jnp.float32),
        down_other,
    )
    first_out = lax.psum_scatter(
        mixer_term.astype(jnp.bfloat16), "tp", scatter_dimension=1, tiled=True
    )
    expert_summed = lax.psum_scatter(
        flat_term.astype(jnp.bfloat16), "tp", scatter_dimension=1, tiled=True
    )
    half_out = expert_summed.reshape(expert_count, capacity, quarter_width)
    returned = lax.all_to_all(half_out, ("z", "y"), split_axis=0, concat_axis=0, tiled=True)
    route_out = returned.reshape(-1, quarter_width).astype(jnp.float32)
    picked = route_out[positions].reshape(row_count, 2, quarter_width)
    shares = jax.nn.sigmoid(route_logits - route_logits[:, ::-1])
    second_out = jnp.sum(picked * shares[:, :, None], axis=1).astype(jnp.bfloat16)
    return (first_out, second_out)


def solution(mesh):
    split_mesh = Mesh(mesh.devices.reshape(8, 4, 2, 4), ("z", "y", "core", "tp"))
    ep = ("z", "y", "core")
    placed = (
        P(ep, None),
        P(),
        P(None, "tp"),
        P("tp", None, None),
        P("tp"),
        P("tp", None),
        P(ep, None),
        P(),
        P(ep, None),
        P(ep, None),
        P(ep, None, "tp"),
        P(ep, None, "tp"),
        P(ep, "tp", None),
    )
    return jax.shard_map(
        local,
        mesh=split_mesh,
        in_specs=placed,
        out_specs=(P(ep, "tp"), P(ep, "tp")),
        check_vma=False,
    )
```

profile of v0, /device:TPU:8, one launch (start us, length us, event | category | flops | bytes accessed | tf_op | source)
XLA Modules:
  0.0 189.3 jit_solution(17867324479856150440)
XLA Ops:
  7.3 3.0 %convert_element_type.81 = f32[256,2048]{1,0:T(8,128)} convert(bf16[256,2048]{1,0:T(8,128)(2,1)} %param.19) | non-fusion elementwise | flops 524288 | bytes 3145728 | tf_op jit(solution)/shard_map/convert_element_type | solution.py:16
  11.1 1.2 fusion.16
  12.7 1.2 reduce-window.6
  14.6 2.6 %scatter_custom_fusion = bf16[576,512]{1,0:T(8,128)(2,1)S(1)} fusion(s32[512]{0:T(512)S(1)} %bitcast.40, bf16[512,512]{1,0:T(8,128)(2,1)S(1)} %reshape.116, bf16[]{:T(256)} %constant.77.clone.1), kind=kCustom, calls=%fused_computation.60 | custom fusion | bytes 589826 | tf_op jit(solution)/shard_map/scatter | solution.py:97
  17.3 33.9 %all_to_all.10 = bf16[32,18,512]{2,1,0:T(8,128)(2,1)S(1)} all-to-all(bf16[32,18,512]{2,1,0:T(8,128)(2,1)S(1)} %reshape.99), channel_id=1, replica_groups=mesh['z'=8,'y'=4,'core'=2,'tp'=4] {'z','y'}, dimensions={0} | all-to-all | bytes 1179648 | tf_op jit(solution)/shard_map/all_to_all | solution.py:100
  51.3 1.0 reshape.100
  53.0 31.6 %all-gather.2.cloned.1.call-done = bf16[576,2048]{1,0:T(8,128)(2,1)} async-done(((bf16[576,512]{1,0:T(8,128)(2,1)}), bf16[576,2048]{1,0:T(8,128)(2,1)}) %all-gather.2.cloned.1.call-update) | async-done | bytes 2359312 | tf_op jit(solution)/shard_map/all_gather | solution.py:102
  84.6 4.9 %fusion.80 = f32[576,512]{1,0:T(8,128)} fusion(bf16[576,2048]{1,0:T(8,128)(2,1)} %all-gather.2.cloned.1.call-done, bf16[1,2048,512]{2,1,0:T(8,128)(2,1)} %param.23), kind=kOutput, calls=%fused_computation.98 | convolution fusion | flops 1207959552 | bytes 5636096 | tf_op jit(solution)/shard_map/dot_general | solution.py:104
  89.5 4.0 %fusion.88 = f32[576,512]{1,0:T(8,128)} fusion(bf16[576,2048]{1,0:T(8,128)(2,1)S(1)} %copy-done.7, bf16[2048,512]{1,0:T(8,128)(2,1)} %collective-permute-done.1), kind=kOutput, calls=%fused_computation.104 | convolution fusion | flops 1207959552 | bytes 5636096 | tf_op jit(solution)/shard_map/dot_general | solution.py:108
  93.5 7.4 %fusion.12 = f32[576,2048]{1,0:T(8,128)} fusion(bf16[576,2048]{1,0:T(8,128)(2,1)S(1)} %copy-done.7, f32[576,512]{1,0:T(8,128)} %fusion.80, bf16[1,512,2048]{2,1,0:T(8,128)(2,1)} %param.25, bf16[1,2048,512]{2,1,0:T(8,128)(2,1)} %param.24), kind=kOutput, calls=%fused_computation.20 | convolution fusion | flops 2417688576 | bytes 12451840 | tf_op jit(solution)/shard_map/dot_general | solution.py:45
  100.9 8.1 %add_convert_fusion = bf16[576,2048]{1,0:T(8,128)(2,1)} fusion(f32[576,2048]{1,0:T(8,128)} %fusion.12, bf16[512,2048]{1,0:T(8,128)(2,1)} %collective-permute-done.3, f32[576,512]{1,0:T(8,128)} %fusion.88, bf16[576,2048]{1,0:T(8,128)(2,1)S(1)} %copy-done.7, bf16[2048,512]{1,0:T(8,128)(2,1)} %collective-permute-done.2), kind=kOutput, calls=%fused_computation.4 | convolution fusion | flops 2420047872 | bytes 14811136 | tf_op jit(solution)/shard_map/dot_general | solution.py:45
  109.1 0.6 copy-done.5
  109.7 0.9 copy-done.2
  111.2 0.8 fusion.8
  112.0 1.9 %collective-permute-start = (bf16[15,256]{1,0:T(8,128)(2,1)S(1)}, bf16[15,256]{1,0:T(8,128)(2,1)S(1)}, u32[]{:S(2)}, u32[]{:S(2)}) collective-permute-start(bf16[15,256]{1,0:T(8,128)(2,1)S(1)} %slice.78), channel_id=1, source_target_pairs={{0,4},{4,8},{8,12},{12,16},{16,20},{20,24},{24,28},{28,32},{32,36}... | collective-permute-start | bytes 23048 | tf_op jit(solution)/shard_map/ppermute | solution.py:12
  114.0 3.0 %collective-permute-done = bf16[15,256]{1,0:T(8,128)(2,1)S(1)} collective-permute-done((bf16[15,256]{1,0:T(8,128)(2,1)S(1)}, bf16[15,256]{1,0:T(8,128)(2,1)S(1)}, u32[]{:S(2)}, u32[]{:S(2)}) %collective-permute-start) | collective-permute-done | bytes 7712 | tf_op jit(solution)/shard_map/ppermute | solution.py:12
  117.0 3.5 %convolution_convert_fusion = bf16[512,2048]{1,0:T(8,128)(2,1)} fusion(bf16[256,2048]{1,0:T(8,128)(2,1)S(1)} %copy-done, f32[256]{0:T(256)S(1)} %convert_element_type.77, bf16[512,256]{1,0:T(8,128)(2,1)S(1)} %fusion.8, f32[527,256]{1,0:T(8,128)S(1)} %maximum_convert_fusion, f32[512]{0:T(512)S(1)} %minimum_convert_fusion, pred[]{:T(512)S(6)} %gt.63, ...), kind=kOutput, calls=%fused_computation.8 | convolution fusion | flops 609878016 | bytes 11930640 | tf_op jit(solution)/shard_map/dot_general | solution.py:85
  120.5 23.2 %reduce-scatter.5.cloned.1.call-done = bf16[576,512]{1,0:T(8,128)(2,1)} async-done(((bf16[576,2048]{1,0:T(8,128)(2,1)}), bf16[576,512]{1,0:T(8,128)(2,1)}) %reduce-scatter.5.cloned.1.call-update) | async-done | bytes 589840 | tf_op jit(solution)/shard_map/reduce_scatter | solution.py:115
  143.7 2.1 %reshape.101 = bf16[32,18,512]{2,1,0:T(8,128)(2,1)} reshape(bf16[576,512]{1,0:T(8,128)(2,1)} %reduce-scatter.5.cloned.1.call-done) | data formatting | bytes 1179648 | tf_op jit(solution)/shard_map/reshape | solution.py:118
  145.8 10.2 %all-to-all-start.1 = ((bf16[32,18,512]{2,1,0:T(8,128)(2,1)}), bf16[32,18,512]{2,1,0:T(8,128)(2,1)S(1)}, u32[]{:S(2)}, u32[]{:S(2)}) async-start(bf16[32,18,512]{2,1,0:T(8,128)(2,1)} %reshape.101), calls=%async_computation.3 | async-start | bytes 1572864 | tf_op jit(solution)/shard_map/all_to_all | solution.py:119
  156.3 22.1 %all-to-all-done.1 = bf16[32,18,512]{2,1,0:T(8,128)(2,1)S(1)} async-done(((bf16[32,18,512]{2,1,0:T(8,128)(2,1)}), bf16[32,18,512]{2,1,0:T(8,128)(2,1)S(1)}, u32[]{:S(2)}, u32[]{:S(2)}) %all-to-all-start.1) | async-done | bytes 589856 | tf_op jit(solution)/shard_map/all_to_all | solution.py:119
  178.5 1.6 gather_fusion
  180.1 0.6 reshape.102
  180.8 2.1 %multiply_reduce_fusion.1 = bf16[256,512]{1,0:T(8,128)(2,1)} fusion(f32[256,2,512]{2,1,0:T(2,128)S(1)} %reshape.102, f32[256,2]{1,0:T(8,128)S(1)} %copy.20), kind=kLoop, calls=%fused_computation.19 | loop fusion | flops 393216 | bytes 1312768 | tf_op jit(solution)/shard_map/reduce_sum | solution.py:123
  (63 shorter events, 4.0 us)
Async XLA Ops:
  7.2 109.8 %copy-start = (bf16[256,2048]{1,0:T(8,128)(2,1)S(1)}, bf16[256,2048]{1,0:T(8,128)(2,1)}, u32[]{:S(2)}) copy-start(bf16[256,2048]{1,0:T(8,128)(2,1)} %param.18) | copy-start | bytes 3145732
  7.2 3.0 %copy-start.1 = (bf16[256,2048]{1,0:T(8,128)(2,1)S(1)}, bf16[256,2048]{1,0:T(8,128)(2,1)}, u32[]{:S(2)}) copy-start(bf16[256,2048]{1,0:T(8,128)(2,1)} %param.19) | copy-start | bytes 3145732
  7.2 77.5 %all-gather.2.cloned.1.call-start = ((), (), s32[]{:S(2)}) async-start(), calls=%async_computation.5 | async-start | bytes 2949120 | tf_op jit(solution)/shard_map/all_gather | solution.py:102
  7.2 3.3 %copy-start.3 = (s32[256,2]{0,1:T(2,128)S(1)}, s32[256,2]{0,1:T(2,128)}, u32[]{:S(2)}) copy-start(s32[256,2]{0,1:T(2,128)} %param.21) | copy-start | bytes 6148
  7.2 3.7 %copy-start.6 = (bf16[2048]{0:T(1024)(128)(2,1)S(1)}, bf16[2048]{0:T(1024)(128)(2,1)}, u32[]{:S(2)}) copy-start(bf16[2048]{0:T(1024)(128)(2,1)} %param.20) | copy-start | bytes 12292
  52.3 91.4 %reduce-scatter.5.cloned.1.call-start = ((), (), s32[]{:S(2)}) async-start(), calls=%async_computation.6 | async-start | bytes 2949120 | tf_op jit(solution)/shard_map/reduce_scatter | solution.py:115
  52.3 37.2 %collective-permute-start.1 = (bf16[2048,512]{1,0:T(8,128)(2,1)}, bf16[2048,512]{1,0:T(8,128)(2,1)}, u32[]{:S(2)}, u32[]{:S(2)}) collective-permute-start(bf16[2048,512]{1,0:T(8,128)(2,1)} %bitcast.43), channel_id=1, source_target_pairs={{0,4},{4,0},{1,5},{5,1},{2,6},{6,2},{3,7},{7,3},{8,12},{12,8},{9,1... | collective-permute-start | bytes 6291464 | tf_op jit(solution)/shard_map/ppermute | solution.py:68
  52.4 48.5 %collective-permute-start.2 = (bf16[2048,512]{1,0:T(8,128)(2,1)}, bf16[2048,512]{1,0:T(8,128)(2,1)}, u32[]{:S(2)}, u32[]{:S(2)}) collective-permute-start(bf16[2048,512]{1,0:T(8,128)(2,1)} %bitcast.44), channel_id=1, source_target_pairs={{0,4},{4,0},{1,5},{5,1},{2,6},{6,2},{3,7},{7,3},{8,12},{12,8},{9,1... | collective-permute-start | bytes 6291464 | tf_op jit(solution)/shard_map/ppermute | solution.py:69
  52.9 48.0 %collective-permute-start.3 = (bf16[512,2048]{1,0:T(8,128)(2,1)}, bf16[512,2048]{1,0:T(8,128)(2,1)}, u32[]{:S(2)}, u32[]{:S(2)}) collective-permute-start(bf16[512,2048]{1,0:T(8,128)(2,1)} %bitcast.45), channel_id=1, source_target_pairs={{0,4},{4,0},{1,5},{5,1},{2,6},{6,2},{3,7},{7,3},{8,12},{12,8},{9,1... | collective-permute-start | bytes 6291464 | tf_op jit(solution)/shard_map/ppermute | solution.py:70
  84.6 4.9 %copy-start.7 = (bf16[576,2048]{1,0:T(8,128)(2,1)S(1)}, bf16[576,2048]{1,0:T(8,128)(2,1)}, u32[]{:S(2)}) copy-start(bf16[576,2048]{1,0:T(8,128)(2,1)} %all-gather.2.cloned.1.call-done) | copy-start | bytes 7077892
  109.0 0.7 copy-start.5
  109.0 1.6 copy-start.2
  109.1 73.8 %reduce-scatter.3.cloned.1.call-start = ((), (), s32[]{:S(2)}) async-start(), calls=%async_computation.4 | async-start | bytes 2621440 | tf_op jit(solution)/shard_map/reduce_scatter | solution.py:112
  109.7 1.4 copy-start.8
  111.1 2.8 %copy-start.10 = (bf16[256]{0:T(256)(128)(2,1)S(1)}, bf16[256]{0:T(256)(128)(2,1)}, u32[]{:S(2)}) copy-start(bf16[256]{0:T(256)(128)(2,1)} %param.17) | copy-start | bytes 1540
  111.2 5.9 %copy-start.9 = (bf16[1,256,256]{2,1,0:T(8,128)(2,1)S(1)}, bf16[1,256,256]{2,1,0:T(8,128)(2,1)}, u32[]{:S(2)}) copy-start(bf16[1,256,256]{2,1,0:T(8,128)(2,1)} %param.16) | copy-start | bytes 393220
  112.0 5.0 %collective-permute-start = (bf16[15,256]{1,0:T(8,128)(2,1)S(1)}, bf16[15,256]{1,0:T(8,128)(2,1)S(1)}, u32[]{:S(2)}, u32[]{:S(2)}) collective-permute-start(bf16[15,256]{1,0:T(8,128)(2,1)S(1)} %slice.78), channel_id=1, source_target_pairs={{0,4},{4,8},{8,12},{12,16},{16,20},{20,24},{24,28},{28,32},{32,36}... | collective-permute-start | bytes 23048 | tf_op jit(solution)/shard_map/ppermute | solution.py:12
  120.5 35.5 %copy-start.4 = (f32[256,2]{0,1:T(2,128)S(1)}, f32[256,2]{0,1:T(2,128)}, u32[]{:S(2)}) copy-start(f32[256,2]{0,1:T(2,128)} %param.22) | copy-start | bytes 6148
  145.8 32.5 %all-to-all-start.1 = ((bf16[32,18,512]{2,1,0:T(8,128)(2,1)}), bf16[32,18,512]{2,1,0:T(8,128)(2,1)S(1)}, u32[]{:S(2)}, u32[]{:S(2)}) async-start(bf16[32,18,512]{2,1,0:T(8,128)(2,1)} %reshape.101), calls=%async_computation.3 | async-start | bytes 1572864 | tf_op jit(solution)/shard_map/all_to_all | solution.py:119
Sparse Core Ops, SparseCore 0:
  52.4 32.2 all-gather.1
  109.2 34.4 reduce-scatter.4
  146.8 31.9 reduce-scatter.2
where the time goes:
time: 190 us; the launch traced here: 189 us
  waiting for transfers between devices  79.9 us (42%)
  blocking collectives  33.9 us (18%)
  matrix products  28.7 us (15%)
  between operations  14.1 us (7%)
  starting transfers between devices  12.9 us (7%)
  local copies, waits for them, and re-layouts  11.5 us (6%)
  other arithmetic  8.35 us (4%)
    all_to_all x1, blocking collectives, local(): lax.all_to_all(buffer, ('z', 'y'), split_axis=0, concat_axis=0, tiled=True)  33.9 us
    all_gather x1, waiting for transfers between devices, local(): portion = lax.all_gather(flattened, 'tp', axis=1, tiled=True)  31.6 us
    reduce_scatter x1, waiting for transfers between devices, local(): lax.psum_scatter(flat_term.astype(jnp.bfloat16), 'tp', scatter_dimension=...  23.2 us
    all_to_all x1, waiting for transfers between devices, local(): lax.all_to_all(half_out, ('z', 'y'), split_axis=0, concat_axis=0, tiled=T...  22.1 us
    dot_general x2, matrix products, expert_output(): return jnp.dot(hidden, down_rows, preferred_element_type=jnp.float32)  15.5 us
    all_to_all x1, starting transfers between devices, local(): lax.all_to_all(half_out, ('z', 'y'), split_axis=0, concat_axis=0, tiled=T...  10.2 us
    dot_general x1, matrix products, local(): jnp.dot(portion, expert_gate[0], preferred_element_type=jnp.float32)  4.89 us
    dot_general x1, matrix products, local(): jnp.dot(portion, gate_other, preferred_element_type=jnp.float32)  3.97 us
  transfers between devices with their start and end apart: 8, of which 4 were waited for; matrix products, arithmetic and copies ran while one was open for 15% of the time, Pallas kernels for 0%

commit v1 on v0

--- a/solution.py
+++ b/solution.py
@@ -99,7 +99,9 @@
     )
     arrived = lax.all_to_all(buffer, ("z", "y"), split_axis=0, concat_axis=0, tiled=True)
     flattened = arrived.reshape(-1, quarter_width)
-    portion = lax.all_gather(flattened, "tp", axis=1, tiled=True)
+    portion = jnp.concatenate(
+        lax.all_to_all(jnp.stack([flattened] * lax.axis_size("tp")), "tp", 0, 0), axis=1
+    )
     flat_term = expert_output(
         jnp.dot(portion, expert_gate[0], preferred_element_type=jnp.float32),
         jnp.dot(portion, expert_up[0], preferred_element_type=jnp.float32),

time: 190 us -> 184 us (0.968)
  waiting for transfers between devices: 79.9 us -> 70.4 us
  starting transfers between devices: 12.9 us -> 17 us
  local copies, waits for them, and re-layouts: 11.5 us -> 14.7 us
  other arithmetic: 8.35 us -> 5.95 us
    all_gather x1 -> x0, waiting for transfers between devices: 31.6 us -> none  [local(): portion = lax.all_gather(flattened, 'tp', axis=1, tiled=True)]
    all_to_all x0 -> x1, waiting for transfers between devices: none -> 26.9 us  [local(): lax.all_to_all(jnp.stack([flattened] * lax.axis_size('tp')), 'tp', 0, 0)]
    reduce_scatter x1, waiting for transfers between devices: 23.2 us -> 18.4 us  [local(): lax.psum_scatter(flat_term.astype(jnp.bfloat16), 'tp', scatter_dimension=...]
    all_to_all x0 -> x1, starting transfers between devices: none -> 4.29 us  [local(): lax.all_to_all(jnp.stack([flattened] * lax.axis_size('tp')), 'tp', 0, 0)]
    dot_general x1, matrix products: 4.89 us -> 2.47 us  [local(): jnp.dot(portion, expert_gate[0], preferred_element_type=jnp.float32)]
    unnamed x23 -> x27, local copies, waits for them, and re-layouts: 1.71 us -> 3.81 us
where the time goes in v1:
time: 184 us
  waiting for transfers between devices  70.4 us (38%)
  blocking collectives  33.9 us (18%)
  matrix products  27.1 us (15%)
  starting transfers between devices  17 us (9%)
  local copies, waits for them, and re-layouts  14.7 us (8%)
  between operations  14.4 us (8%)
  other arithmetic  5.95 us (3%)
    all_to_all x1, blocking collectives, local(): lax.all_to_all(buffer, ('z', 'y'), split_axis=0, concat_axis=0, tiled=True)  33.9 us
    all_to_all x1, waiting for transfers between devices, local(): lax.all_to_all(jnp.stack([flattened] * lax.axis_size('tp')), 'tp', 0, 0)  26.9 us
    all_to_all x1, waiting for transfers between devices, local(): lax.all_to_all(half_out, ('z', 'y'), split_axis=0, concat_axis=0, tiled=T...  22.1 us
    reduce_scatter x1, waiting for transfers between devices, local(): lax.psum_scatter(flat_term.astype(jnp.bfloat16), 'tp', scatter_dimension=...  18.4 us
    dot_general x2, matrix products, expert_output(): return jnp.dot(hidden, down_rows, preferred_element_type=jnp.float32)  16.4 us
    all_to_all x1, starting transfers between devices, local(): lax.all_to_all(half_out, ('z', 'y'), split_axis=0, concat_axis=0, tiled=T...  10.2 us
    all_to_all x1, starting transfers between devices, local(): lax.all_to_all(jnp.stack([flattened] * lax.axis_size('tp')), 'tp', 0, 0)  4.29 us
    dot_general x1, matrix products, local(): jnp.dot(portion, gate_other, preferred_element_type=jnp.float32)  3.99 us
  transfers between devices with their start and end apart: 8, of which 4 were waited for; matrix products, arithmetic and copies ran while one was open for 15% of the time, Pallas kernels for 0%

profile of v1, /device:TPU:8, one launch (start us, length us, event | category | flops | bytes accessed | tf_op | source)
XLA Modules:
  0.0 183.6 jit_solution(6292548652725823668)
XLA Ops:
  7.2 1.6 convert_element_type.81
  10.3 1.2 reduce-window.6
  12.1 2.6 %scatter_custom_fusion = bf16[576,512]{1,0:T(8,128)(2,1)S(1)} fusion(s32[512]{0:T(512)S(1)} %bitcast.48, bf16[512,512]{1,0:T(8,128)(2,1)S(1)} %reshape.122, bf16[]{:T(256)} %constant.77.clone.1), kind=kCustom, calls=%fused_computation.60 | custom fusion | bytes 589826 | tf_op jit(solution)/shard_map/scatter | solution.py:97
  14.9 33.9 %all_to_all.15 = bf16[32,18,512]{2,1,0:T(8,128)(2,1)S(1)} all-to-all(bf16[32,18,512]{2,1,0:T(8,128)(2,1)S(1)} %reshape.104), channel_id=1, replica_groups=mesh['z'=8,'y'=4,'core'=2,'tp'=4] {'z','y'}, dimensions={0} | all-to-all | bytes 1179648 | tf_op jit(solution)/shard_map/all_to_all | solution.py:100
  49.0 1.6 stack.3
  50.6 4.3 %all-to-all-start.1 = ((bf16[4,576,512]{2,1,0:T(8,128)(2,1)}), bf16[4,576,512]{2,1,0:T(8,128)(2,1)S(1)}, u32[]{:S(2)}, u32[]{:S(2)}) async-start(bf16[4,576,512]{2,1,0:T(8,128)(2,1)} %stack.3), calls=%async_computation.2 | async-start | bytes 4718592 | tf_op jit(solution)/shard_map/all_to_all | solution.py:103
  55.5 26.9 %all-to-all-done.1 = bf16[4,576,512]{2,1,0:T(8,128)(2,1)S(1)} async-done(((bf16[4,576,512]{2,1,0:T(8,128)(2,1)}), bf16[4,576,512]{2,1,0:T(8,128)(2,1)S(1)}, u32[]{:S(2)}, u32[]{:S(2)}) %all-to-all-start.1) | async-done | bytes 2359328 | tf_op jit(solution)/shard_map/all_to_all | solution.py:103
  82.7 2.1 %copy-done.9 = bf16[1,2048,512]{2,1,0:T(8,128)(2,1)S(1)} copy-done((bf16[1,2048,512]{2,1,0:T(8,128)(2,1)S(1)}, bf16[1,2048,512]{2,1,0:T(8,128)(2,1)}, u32[]{:S(2)}) %copy-start.9) | copy-done | bytes 2097176
  84.8 2.5 %fusion.80 = f32[576,512]{1,0:T(8,128)} fusion(bf16[576,2048]{1,0:T(8,128)(2,1)S(1)} %bitcast.44, bf16[1,2048,512]{2,1,0:T(8,128)(2,1)S(1)} %copy-done.9), kind=kOutput, calls=%fused_computation.98 | convolution fusion | flops 1207959552 | bytes 5636096 | tf_op jit(solution)/shard_map/dot_general | solution.py:106
  87.3 4.0 %fusion.88 = f32[576,512]{1,0:T(8,128)} fusion(bf16[576,2048]{1,0:T(8,128)(2,1)S(1)} %bitcast.45, bf16[2048,512]{1,0:T(8,128)(2,1)} %collective-permute-done.1), kind=kOutput, calls=%fused_computation.104 | convolution fusion | flops 1207959552 | bytes 5636096 | tf_op jit(solution)/shard_map/dot_general | solution.py:110
  91.3 8.3 %fusion.12 = f32[576,2048]{1,0:T(8,128)} fusion(bf16[576,2048]{1,0:T(8,128)(2,1)} %bitcast.46, f32[576,512]{1,0:T(8,128)} %fusion.80, bf16[1,512,2048]{2,1,0:T(8,128)(2,1)} %param.25, bf16[1,2048,512]{2,1,0:T(8,128)(2,1)} %param.24), kind=kOutput, calls=%fused_computation.20 | convolution fusion | flops 2417688576 | bytes 12451840 | tf_op jit(solution)/shard_map/dot_general | solution.py:45
  99.6 8.1 %add_convert_fusion = bf16[576,2048]{1,0:T(8,128)(2,1)} fusion(f32[576,2048]{1,0:T(8,128)} %fusion.12, bf16[512,2048]{1,0:T(8,128)(2,1)} %collective-permute-done.3, f32[576,512]{1,0:T(8,128)} %fusion.88, bf16[576,2048]{1,0:T(8,128)(2,1)S(1)} %bitcast.47, bf16[2048,512]{1,0:T(8,128)(2,1)} %collective-permute-done.2), kind=kOutput, calls=%fused_computation.4 | convolution fusion | flops 2420047872 | bytes 14811136 | tf_op jit(solution)/shard_map/dot_general | solution.py:45
  108.4 0.9 copy-done.4
  109.8 0.8 fusion.8
  110.6 1.9 %collective-permute-start = (bf16[15,256]{1,0:T(8,128)(2,1)S(1)}, bf16[15,256]{1,0:T(8,128)(2,1)S(1)}, u32[]{:S(2)}, u32[]{:S(2)}) collective-permute-start(bf16[15,256]{1,0:T(8,128)(2,1)S(1)} %slice.78), channel_id=1, source_target_pairs={{0,4},{4,8},{8,12},{12,16},{16,20},{20,24},{24,28},{28,32},{32,36}... | collective-permute-start | bytes 23048 | tf_op jit(solution)/shard_map/ppermute | solution.py:12
  112.6 3.0 %collective-permute-done = bf16[15,256]{1,0:T(8,128)(2,1)S(1)} collective-permute-done((bf16[15,256]{1,0:T(8,128)(2,1)S(1)}, bf16[15,256]{1,0:T(8,128)(2,1)S(1)}, u32[]{:S(2)}, u32[]{:S(2)}) %collective-permute-start) | collective-permute-done | bytes 7712 | tf_op jit(solution)/shard_map/ppermute | solution.py:12
  115.7 3.5 %convolution_convert_fusion = bf16[512,2048]{1,0:T(8,128)(2,1)} fusion(bf16[256,2048]{1,0:T(8,128)(2,1)S(1)} %copy-done, f32[256]{0:T(256)S(1)} %convert_element_type.77, bf16[512,256]{1,0:T(8,128)(2,1)S(1)} %fusion.8, f32[527,256]{1,0:T(8,128)S(1)} %maximum_convert_fusion, f32[512]{0:T(512)S(1)} %minimum_convert_fusion, pred[]{:T(512)S(6)} %gt.63, ...), kind=kOutput, calls=%fused_computation.8 | convolution fusion | flops 609878016 | bytes 11930640 | tf_op jit(solution)/shard_map/dot_general | solution.py:85
  119.2 18.4 %reduce-scatter.5.cloned.1.call-done = bf16[576,512]{1,0:T(8,128)(2,1)} async-done(((bf16[576,2048]{1,0:T(8,128)(2,1)}), bf16[576,512]{1,0:T(8,128)(2,1)}) %reduce-scatter.5.cloned.1.call-update) | async-done | bytes 589840 | tf_op jit(solution)/shard_map/reduce_scatter | solution.py:117
  137.6 2.1 %reshape.107 = bf16[32,18,512]{2,1,0:T(8,128)(2,1)} reshape(bf16[576,512]{1,0:T(8,128)(2,1)} %reduce-scatter.5.cloned.1.call-done) | data formatting | bytes 1179648 | tf_op jit(solution)/shard_map/reshape | solution.py:120
  139.7 10.2 %all-to-all-start.2 = ((bf16[32,18,512]{2,1,0:T(8,128)(2,1)}), bf16[32,18,512]{2,1,0:T(8,128)(2,1)S(1)}, u32[]{:S(2)}, u32[]{:S(2)}) async-start(bf16[32,18,512]{2,1,0:T(8,128)(2,1)} %reshape.107), calls=%async_computation.4 | async-start | bytes 1572864 | tf_op jit(solution)/shard_map/all_to_all | solution.py:121
  150.1 22.1 %all-to-all-done.2 = bf16[32,18,512]{2,1,0:T(8,128)(2,1)S(1)} async-done(((bf16[32,18,512]{2,1,0:T(8,128)(2,1)}), bf16[32,18,512]{2,1,0:T(8,128)(2,1)S(1)}, u32[]{:S(2)}, u32[]{:S(2)}) %all-to-all-start.2) | async-done | bytes 589856 | tf_op jit(solution)/shard_map/all_to_all | solution.py:121
  172.4 1.6 gather_fusion
  174.0 0.6 reshape.108
  174.7 2.1 %multiply_reduce_fusion.1 = bf16[256,512]{1,0:T(8,128)(2,1)} fusion(f32[256,2,512]{2,1,0:T(2,128)S(1)} %reshape.108, f32[256,2]{1,0:T(8,128)S(1)} %copy.26), kind=kLoop, calls=%fused_computation.19 | loop fusion | flops 393216 | bytes 1312768 | tf_op jit(solution)/shard_map/reduce_sum | solution.py:125
  (68 shorter events, 5.0 us)
Async XLA Ops:
  7.2 108.5 %copy-start = (bf16[256,2048]{1,0:T(8,128)(2,1)S(1)}, bf16[256,2048]{1,0:T(8,128)(2,1)}, u32[]{:S(2)}) copy-start(bf16[256,2048]{1,0:T(8,128)(2,1)} %param.18) | copy-start | bytes 3145732
  7.2 1.6 copy-start.1
  7.2 1.9 %copy-start.5 = (s32[256,2]{0,1:T(2,128)S(1)}, s32[256,2]{0,1:T(2,128)}, u32[]{:S(2)}) copy-start(s32[256,2]{0,1:T(2,128)} %param.21) | copy-start | bytes 6148
  7.2 2.4 %copy-start.8 = (bf16[2048]{0:T(1024)(128)(2,1)S(1)}, bf16[2048]{0:T(1024)(128)(2,1)}, u32[]{:S(2)}) copy-start(bf16[2048]{0:T(1024)(128)(2,1)} %param.20) | copy-start | bytes 12292
  50.6 31.8 %all-to-all-start.1 = ((bf16[4,576,512]{2,1,0:T(8,128)(2,1)}), bf16[4,576,512]{2,1,0:T(8,128)(2,1)S(1)}, u32[]{:S(2)}, u32[]{:S(2)}) async-start(bf16[4,576,512]{2,1,0:T(8,128)(2,1)} %stack.3), calls=%async_computation.2 | async-start | bytes 4718592 | tf_op jit(solution)/shard_map/all_to_all | solution.py:103
  54.9 82.7 %reduce-scatter.5.cloned.1.call-start = ((), (), s32[]{:S(2)}) async-start(), calls=%async_computation.6 | async-start | bytes 2949120 | tf_op jit(solution)/shard_map/reduce_scatter | solution.py:117
  54.9 32.4 %collective-permute-start.1 = (bf16[2048,512]{1,0:T(8,128)(2,1)}, bf16[2048,512]{1,0:T(8,128)(2,1)}, u32[]{:S(2)}, u32[]{:S(2)}) collective-permute-start(bf16[2048,512]{1,0:T(8,128)(2,1)} %bitcast.51), channel_id=1, source_target_pairs={{0,4},{4,0},{1,5},{5,1},{2,6},{6,2},{3,7},{7,3},{8,12},{12,8},{9,1... | collective-permute-start | bytes 6291464 | tf_op jit(solution)/shard_map/ppermute | solution.py:68
  54.9 44.6 %collective-permute-start.2 = (bf16[2048,512]{1,0:T(8,128)(2,1)}, bf16[2048,512]{1,0:T(8,128)(2,1)}, u32[]{:S(2)}, u32[]{:S(2)}) collective-permute-start(bf16[2048,512]{1,0:T(8,128)(2,1)} %bitcast.52), channel_id=1, source_target_pairs={{0,4},{4,0},{1,5},{5,1},{2,6},{6,2},{3,7},{7,3},{8,12},{12,8},{9,1... | collective-permute-start | bytes 6291464 | tf_op jit(solution)/shard_map/ppermute | solution.py:69
  55.4 44.1 %collective-permute-start.3 = (bf16[512,2048]{1,0:T(8,128)(2,1)}, bf16[512,2048]{1,0:T(8,128)(2,1)}, u32[]{:S(2)}, u32[]{:S(2)}) collective-permute-start(bf16[512,2048]{1,0:T(8,128)(2,1)} %bitcast.53), channel_id=1, source_target_pairs={{0,4},{4,0},{1,5},{5,1},{2,6},{6,2},{3,7},{7,3},{8,12},{12,8},{9,1... | collective-permute-start | bytes 6291464 | tf_op jit(solution)/shard_map/ppermute | solution.py:70
  82.4 2.4 %copy-start.9 = (bf16[1,2048,512]{2,1,0:T(8,128)(2,1)S(1)}, bf16[1,2048,512]{2,1,0:T(8,128)(2,1)}, u32[]{:S(2)}) copy-start(bf16[1,2048,512]{2,1,0:T(8,128)(2,1)} %param.23) | copy-start | bytes 6291460
  82.7 4.6 %copy-start.2 = (bf16[4,72,8,512]{3,2,0,1:T(8,128)(2,1)}, bf16[4,72,8,512]{3,2,0,1:T(8,128)(2,1)S(1)}, u32[]{:S(2)}) copy-start(bf16[4,72,8,512]{3,2,0,1:T(8,128)(2,1)S(1)} %copy.28) | copy-start | bytes 7077892
  91.3 8.3 %copy-start.3 = (bf16[4,72,8,512]{3,2,0,1:T(8,128)(2,1)S(1)}, bf16[4,72,8,512]{3,2,0,1:T(8,128)(2,1)}, u32[]{:S(2)}) copy-start(bf16[4,72,8,512]{3,2,0,1:T(8,128)(2,1)} %copy-done.2) | copy-start | bytes 7077892
  107.7 0.7 copy-start.7
  107.7 1.6 copy-start.4
  107.7 69.0 %reduce-scatter.3.cloned.1.call-start = ((), (), s32[]{:S(2)}) async-start(), calls=%async_computation.5 | async-start | bytes 2621440 | tf_op jit(solution)/shard_map/reduce_scatter | solution.py:114
  108.4 1.4 copy-start.10
  109.8 2.8 %copy-start.12 = (bf16[256]{0:T(256)(128)(2,1)S(1)}, bf16[256]{0:T(256)(128)(2,1)}, u32[]{:S(2)}) copy-start(bf16[256]{0:T(256)(128)(2,1)} %param.17) | copy-start | bytes 1540
  109.8 5.9 %copy-start.11 = (bf16[1,256,256]{2,1,0:T(8,128)(2,1)S(1)}, bf16[1,256,256]{2,1,0:T(8,128)(2,1)}, u32[]{:S(2)}) copy-start(bf16[1,256,256]{2,1,0:T(8,128)(2,1)} %param.16) | copy-start | bytes 393220
  110.6 5.0 %collective-permute-start = (bf16[15,256]{1,0:T(8,128)(2,1)S(1)}, bf16[15,256]{1,0:T(8,128)(2,1)S(1)}, u32[]{:S(2)}, u32[]{:S(2)}) collective-permute-start(bf16[15,256]{1,0:T(8,128)(2,1)S(1)} %slice.78), channel_id=1, source_target_pairs={{0,4},{4,8},{8,12},{12,16},{16,20},{20,24},{24,28},{28,32},{32,36}... | collective-permute-start | bytes 23048 | tf_op jit(solution)/shard_map/ppermute | solution.py:12
  119.2 30.7 %copy-start.6 = (f32[256,2]{0,1:T(2,128)S(1)}, f32[256,2]{0,1:T(2,128)}, u32[]{:S(2)}) copy-start(f32[256,2]{0,1:T(2,128)} %param.22) | copy-start | bytes 6148
  139.7 32.5 %all-to-all-start.2 = ((bf16[32,18,512]{2,1,0:T(8,128)(2,1)}), bf16[32,18,512]{2,1,0:T(8,128)(2,1)S(1)}, u32[]{:S(2)}, u32[]{:S(2)}) async-start(bf16[32,18,512]{2,1,0:T(8,128)(2,1)} %reshape.107), calls=%async_computation.4 | async-start | bytes 1572864 | tf_op jit(solution)/shard_map/all_to_all | solution.py:121
Sparse Core Ops, SparseCore 0:
  107.8 29.7 reduce-scatter.4
  140.7 32.0 reduce-scatter.2
